TPU v7x, 32 devices: a whole 2x2x4 slice. The times are simulated.
32 devices in a mesh: grp: 2 (over y), sp: 4 (over z), tp: 4 (over x, core).
Axes of the slice: x: 2, y: 2, z: 4, core: 2. Of those that a mesh axis runs over, the one named last changes fastest.
Arguments:
- query_nope: bfloat16 [2560, 1024], P(('grp', 'sp'), 'tp'), parts along dimension 0, may hold values from -12 to 12
- query_rope: bfloat16 [2560, 512], P(('grp', 'sp'), 'tp'), parts along dimension 0, may hold values from -48 to 48
- token_latent: bfloat16 [2560, 256], P(('grp', 'sp')), parts along dimension 0, may hold values from -6 to 6
- key_rope: bfloat16 [2560, 32], P(('grp', 'sp')), parts along dimension 0, may hold values from -48 to 48
- latent_norm_gain: float32 [256], replicated, may hold values from 0.1 to 1.9
- key_expand_weight: bfloat16 [256, 1024], replicated, may hold values from -0.375 to 0.375
- value_expand_weight: bfloat16 [256, 1024], replicated, may hold values from -0.375 to 0.375
- residual: bfloat16 [2560, 2048], P(('grp', 'sp')), parts along dimension 0, may hold values from -3 to 3
- out_weight: bfloat16 [1024, 2048], P('tp'), may hold values from -0.375 to 0.375
- ffn_gain: float32 [2048], replicated, may hold values from 0.1 to 1.9
- gate_weight: bfloat16 [2048, 5632], P('sp', 'tp'), may hold values from -0.125 to 0.125
- up_weight: bfloat16 [2048, 5632], P('sp', 'tp'), may hold values from -0.125 to 0.125
- down_weight: bfloat16 [5632, 2048], P('tp', 'sp'), may hold values from -0.078125 to 0.078125
Outputs:
- layer_output: bfloat16 [2560, 2048], P(('grp', 'sp', 'tp')), parts along dimension 0
There are 2 independent parts, one for each index of `grp`. A program takes and returns all parts, laid end to end along the dimension named above; an argument that names none is the same for every part. Nothing has to cross between parts.
All inputs are finite; a program needn't handle non-finite values.
Results may differ from a plain program's by a relative error of at most 0.015.
Values may be sent and summed in bfloat16 or wider, within the bound.
A program may use at most 128 MiB of HBM per device.

v0:
```python
import jax
import jax.numpy as jnp
from jax import lax
from jax.sharding import PartitionSpec as P

UNROTATED_SIZE = 64
ROPE = 32
VALUE_SIZE = 64
GRID_W = 64


def norm_rows(values, gain):
    wide = values.astype(jnp.float32)
    return wide * lax.rsqrt(jnp.mean(wide * wide, axis=-1, keepdims=True) + 1e-06) * gain


def turn_heads(vectors, positions):
    tokens, heads, width = vectors.shape
    freqs = width // 4
    grid_pos = jnp.stack([positions // GRID_W, positions % GRID_W], axis=-1).astype(jnp.float32)
    inverse = jnp.power(10000.0, -jnp.arange(freqs, dtype=jnp.float32) / freqs)
    angles = grid_pos[:, :, None] * inverse
    cosine = jnp.cos(angles)[:, None]
    sine = jnp.sin(angles)[:, None]
    viewed = vectors.reshape(tokens, heads, 2, 2, freqs)
    first = viewed[..., 0, :]
    second = viewed[..., 1, :]
    turned = jnp.stack([first * cosine - second * sine, first * sine + second * cosine], axis=-2)
    return turned.reshape(tokens, heads, width)


def local(
    query_nope,
    query_rope,
    token_latent,
    key_rope,
    latent_norm_gain,
    key_expand_weight,
    value_expand_weight,
    residual,
    out_weight,
    ffn_gain,
    gate_weight,
    up_weight,
    down_weight,
):
    tok_rows = query_nope.shape[0]
    heads_here = query_nope.shape[1] // UNROTATED_SIZE
    own_rows = tok_rows // lax.axis_size("tp")
    tp_index = lax.axis_index("tp")
    positions = lax.axis_index("sp") * tok_rows + jnp.arange(tok_rows, dtype=jnp.int32)
    query_flat = query_nope.reshape(tok_rows, heads_here, UNROTATED_SIZE)
    query_turned = turn_heads(
        query_rope.astype(jnp.float32).reshape(tok_rows, heads_here, ROPE), positions
    ).astype(jnp.bfloat16)
    latent = norm_rows(token_latent, latent_norm_gain).astype(jnp.bfloat16)
    key_turned = turn_heads(key_rope.astype(jnp.float32)[:, None, :], positions)[:, 0].astype(
        jnp.bfloat16
    )
    key_cols = lax.dynamic_slice_in_dim(
        key_expand_weight, tp_index * heads_here * UNROTATED_SIZE, heads_here * UNROTATED_SIZE, 1
    )
    value_cols = lax.dynamic_slice_in_dim(
        value_expand_weight, tp_index * heads_here * VALUE_SIZE, heads_here * VALUE_SIZE, 1
    )
    score_scale = (UNROTATED_SIZE + ROPE) ** (-0.5)

    def absorb(carried, block_in):
        latent_block, rope_block = block_in
        block_rows = latent_block.shape[0]
        key_rows = jnp.dot(latent_block, key_cols, preferred_element_type=jnp.float32).astype(
            jnp.bfloat16
        )
        key_rows = key_rows.reshape(block_rows, heads_here, UNROTATED_SIZE)
        value_rows = jnp.dot(latent_block, value_cols, preferred_element_type=jnp.float32).astype(
            jnp.bfloat16
        )
        value_rows = value_rows.reshape(block_rows, heads_here, VALUE_SIZE)
        scores = (
            jnp.einsum("qhd,khd->hqk", query_flat, key_rows, preferred_element_type=jnp.float32)
            + jnp.einsum(
                "qhd,kd->hqk", query_turned, rope_block, preferred_element_type=jnp.float32
            )
        ) * score_scale
        highest, totals, accumulated = carried
        new_highest = jnp.maximum(highest, jnp.max(scores, axis=-1))
        shrink = jnp.exp(highest - new_highest)
        weights = jnp.exp(scores - new_highest[:, :, None])
        totals = totals * shrink + jnp.sum(weights, axis=-1)
        accumulated = accumulated * shrink.T[:, :, None] + jnp.einsum(
            "hqk,khd->qhd",
            weights.astype(jnp.bfloat16),
            value_rows,
            preferred_element_type=jnp.float32,
        )
        return ((new_highest, totals, accumulated), None)

    initial = (
        jnp.full((heads_here, tok_rows), -jnp.inf, jnp.float32),
        jnp.zeros((heads_here, tok_rows), jnp.float32),
        jnp.zeros((tok_rows, heads_here, VALUE_SIZE), jnp.float32),
    )
    carried = initial
    latent_piece = lax.all_gather(latent, "sp", axis=0, tiled=True)
    rope_piece = lax.all_gather(key_turned, "sp", axis=0, tiled=True)
    shard_count = latent_piece.shape[0] // tok_rows
    grouped = max(
        (
            factor
            for factor in range(1, shard_count + 1)
            if shard_count % factor == 0 and factor * tok_rows <= max(1024, tok_rows)
        )
    )
    block_rows = grouped * tok_rows
    blocks = (
        latent_piece.reshape(-1, block_rows, latent_piece.shape[1]),
        rope_piece.reshape(-1, block_rows, rope_piece.shape[1]),
    )
    carried, _ = lax.scan(absorb, carried, blocks)
    highest, totals, accumulated = carried
    attended = (
        (accumulated / totals.T[:, :, None])
        .reshape(tok_rows, heads_here * VALUE_SIZE)
        .astype(jnp.bfloat16)
    )
    projected = jnp.dot(attended, out_weight, preferred_element_type=jnp.float32).astype(
        jnp.bfloat16
    )
    summed = lax.psum(projected, "tp").astype(jnp.float32)
    mixed_all = residual.astype(jnp.float32) + summed
    normed_all = norm_rows(mixed_all, ffn_gain).astype(jnp.bfloat16)
    mixed_own = lax.dynamic_slice_in_dim(mixed_all, tp_index * own_rows, own_rows, 0)
    gate_piece = lax.all_gather(gate_weight, "sp", axis=0, tiled=True)
    up_piece = lax.all_gather(up_weight, "sp", axis=0, tiled=True)
    gate = jnp.dot(normed_all, gate_piece, preferred_element_type=jnp.float32)
    up_part = jnp.dot(normed_all, up_piece, preferred_element_type=jnp.float32)
    hidden = (jax.nn.silu(gate) * up_part).astype(jnp.bfloat16)
    terms = jnp.dot(
        hidden,
        lax.all_gather(down_weight, "sp", axis=1, tiled=True),
        preferred_element_type=jnp.float32,
    )
    ffn_own = lax.psum_scatter(
        terms.astype(jnp.bfloat16), "tp", scatter_dimension=0, tiled=True
    ).astype(jnp.float32)
    return (mixed_own + ffn_own).astype(jnp.bfloat16)


def solution(mesh):
    return jax.shard_map(
        local,
        mesh=mesh,
        in_specs=(
            P(("grp", "sp"), "tp"),
            P(("grp", "sp"), "tp"),
            P(("grp", "sp"), None),
            P(("grp", "sp"), None),
            P(),
            P(),
            P(),
            P(("grp", "sp"), None),
            P("tp", None),
            P(),
            P("sp", "tp"),
            P("sp", "tp"),
            P("tp", "sp"),
        ),
        out_specs=P(("grp", "sp", "tp"), None),
        check_vma=False,
    )
```

profile of v0, /device:TPU:0, one launch (start us, length us, event | category | flops | bytes accessed | tf_op | source)
XLA Modules:
  0.0 428.1 jit_solution(11533256106749414533)
XLA Ops:
  7.4 0.0 copy-start
  7.4 0.0 copy-start.3
  7.4 0.0 all-reduce.2.cloned.1.call-start
  7.4 1.1 copy.26
  8.6 0.7 convert.18
  9.3 0.2 multiply_cosine_fusion
  9.5 0.2 fusion.32
  9.7 15.1 %all-gather = bf16[4,320,32]{1,2,0:T(8,128)(2,1)S(1)} all-gather(bf16[1,320,32]{1,2,0:T(8,128)(2,1)S(1)} %bitcast.82), channel_id=1, replica_groups=mesh['grp'=2,'sp'=4,'tp'=4] {'sp'}, dimensions={0}, use_global_device_ids=true | all-gather | bytes 102400 | tf_op jit(solution)/shard_map/all_gather | solution.py:105
  24.8 0.1 copy.25
  24.8 0.1 reshape.160
  25.0 1.1 fusion.24
  26.1 1.0 fusion.26
  27.1 16.8 %all_gather.15 = bf16[1280,256]{1,0:T(8,128)(2,1)S(1)} all-gather(bf16[320,256]{1,0:T(8,128)(2,1)S(1)} %fusion.26), channel_id=1, replica_groups=mesh['grp'=2,'sp'=4,'tp'=4] {'sp'}, dimensions={0}, use_global_device_ids=true | all-gather | bytes 819200 | tf_op jit(solution)/shard_map/all_gather | solution.py:104
  43.9 0.0 copy-done.3
  43.9 0.2 copy.24
  44.2 1.0 constant_dynamic-slice_fusion
  45.2 15.2 %while.15 = (s32[]{:T(128)}, f32[4,320]{1,0:T(4,128)S(1)}, f32[4,320]{1,0:T(4,128)S(1)}, f32[320,4,64]{0,2,1:T(8,128)S(1)}, bf16[2,640,256]{2,1,0:T(8,128)(2,1)S...) while((s32[]{:T(128)}, f32[4,320]{1,0:T(4,128)S(1)}, ...), condition=%wide.region_4.5_spmd.clone, body=%wide.region_1.4_spmd.clone.sunk | while | flops 436231680 | bytes 32759976 | solution.py:119
  45.2 0.3 convolution_convert_fusion.6
  45.5 0.6 fusion.74
  46.1 2.4 fusion.75
  48.5 0.0 copy-start.1
  48.5 0.3 convolution_convert_fusion.7
  48.8 2.9 fusion.79
  51.7 0.0 copy-done.1
  51.8 1.0 fusion.77
  52.8 0.3 convolution_convert_fusion.6
  53.1 0.6 fusion.74
  53.7 2.4 fusion.75
  56.1 0.0 copy-start.1
  56.1 0.3 convolution_convert_fusion.7
  56.4 2.9 fusion.79
  59.3 0.0 copy-done.1
  59.3 1.0 fusion.77
  60.4 0.0 copy-done
  60.4 1.6 convolution_convert_fusion.3
  62.0 0.0 copy-start.2
  62.0 0.0 all-reduce.2.cloned.1.call-update
  62.1 0.0 all-gather.5.cloned.1.call-start
  62.1 0.5 all-gather.5.cloned.1.call-update
  62.6 0.0 all-gather.7.cloned.1.call-start
  62.7 0.5 all-gather.7.cloned.1.call-update
  63.2 0.0 all-gather.9.cloned.1.call-start
  63.3 0.5 all-gather.9.cloned.1.call-update
  63.8 0.0 copy-start.4
  63.8 0.0 reduce-scatter.2.cloned.1.call-start
  63.9 37.3 %all-reduce.2.cloned.1.call-done = bf16[320,2048]{1,0:T(8,128)(2,1)} async-done(((bf16[320,2048]{1,0:T(8,128)(2,1)}), bf16[320,2048]{1,0:T(8,128)(2,1)}) %all-reduce.2.cloned.1.call-update) | async-done | bytes 1310736 | tf_op jit(solution)/shard_map/psum | solution.py:129
  101.1 0.0 copy-done.2
  101.1 3.2 convert_add_fusion
  104.4 66.1 %all-gather.5.cloned.1.call-done = bf16[2048,1408]{1,0:T(8,128)(2,1)} async-done(((bf16[512,1408]{1,0:T(8,128)(2,1)}), bf16[2048,1408]{1,0:T(8,128)(2,1)}) %all-gather.5.cloned.1.call-update) | async-done | bytes 5767184 | tf_op jit(solution)/shard_map/all_gather | solution.py:133
  170.5 0.0 copy-done.4
  170.5 6.5 %fusion.36 = f32[320,1408]{1,0:T(8,128)} fusion(bf16[2048,1408]{1,0:T(8,128)(2,1)} %all-gather.5.cloned.1.call-done, f32[2048]{0:T(1024)S(1)} %copy-done.4, f32[320]{0:T(512)S(1)} %add_rsqrt_fusion, bf16[320,2048]{1,0:T(8,128)(2,1)} %all-reduce.2.cloned.1.call-done, bf16[320,2048]{1,0:T(8,128)(2,1)S(1)} %copy-done.2), kind=kOutput, calls=%fused_computation.69 | convolution fusion | flops 1849425920 | bytes 10200320 | tf_op jit(solution)/shard_map/dot_general | solution.py:135
  177.0 99.7 %all-gather.7.cloned.1.call-done = bf16[2048,1408]{1,0:T(8,128)(2,1)} async-done(((bf16[512,1408]{1,0:T(8,128)(2,1)}), bf16[2048,1408]{1,0:T(8,128)(2,1)}) %all-gather.7.cloned.1.call-update) | async-done | bytes 5767184 | tf_op jit(solution)/shard_map/all_gather | solution.py:134
  276.8 106.3 %all-gather.9.cloned.1.call-done = bf16[1408,2048]{1,0:T(8,128)(2,1)} async-done(((bf16[1408,512]{1,0:T(8,128)(2,1)}), bf16[1408,2048]{1,0:T(8,128)(2,1)}) %all-gather.9.cloned.1.call-update) | async-done | bytes 5767184 | tf_op jit(solution)/shard_map/all_gather | solution.py:140
  383.0 10.7 %convolution_convert_fusion.2 = bf16[320,2048]{1,0:T(8,128)(2,1)} fusion(bf16[1408,2048]{1,0:T(8,128)(2,1)} %all-gather.9.cloned.1.call-done, bf16[2048,1408]{1,0:T(8,128)(2,1)} %all-gather.7.cloned.1.call-done, f32[320,1408]{1,0:T(8,128)} %fusion.36, f32[2048]{0:T(1024)S(1)} %copy-done.4, f32[320]{0:T(512)S(1)} %add_rsqrt_fusion, ...), kind=kOutput, calls=%fused_computation.27 | convolution fusion | flops 3698278400 | bytes 17278208 | tf_op jit(solution)/shard_map/dot_general | solution.py:138
  393.7 0.0 reduce-scatter.2.cloned.1.call-update
  393.7 24.8 %reduce-scatter.2.cloned.1.call-done = bf16[80,2048]{1,0:T(8,128)(2,1)} async-done(((bf16[320,2048]{1,0:T(8,128)(2,1)}), bf16[80,2048]{1,0:T(8,128)(2,1)}) %reduce-scatter.2.cloned.1.call-update) | async-done | bytes 327696 | tf_op jit(solution)/shard_map/reduce_scatter | solution.py:143
  418.6 2.0 add_convert_fusion
  (20 shorter events, 0.3 us)
Async XLA Ops:
  7.4 53.0 %copy-start = (bf16[256,2048]{1,0:T(8,128)(2,1)S(1)}, bf16[256,2048]{1,0:T(8,128)(2,1)}, u32[]{:S(2)}) copy-start(bf16[256,2048]{1,0:T(8,128)(2,1)} %param.23) | copy-start | bytes 3145732
  7.4 36.6 %copy-start.3 = (bf16[320,256]{1,0:T(8,128)(2,1)S(1)}, bf16[320,256]{1,0:T(8,128)(2,1)}, u32[]{:S(2)}) copy-start(bf16[320,256]{1,0:T(8,128)(2,1)} %param.15) | copy-start | bytes 491524
  7.4 93.8 %all-reduce.2.cloned.1.call-start = ((), (), s32[]{:S(2)}) async-start(), calls=%async_computation.1 | async-start | bytes 2621440 | tf_op jit(solution)/shard_map/psum | solution.py:129
  48.5 3.2 copy-start.1
  56.1 3.2 copy-start.1
  62.0 39.1 %copy-start.2 = (bf16[320,2048]{1,0:T(8,128)(2,1)S(1)}, bf16[320,2048]{1,0:T(8,128)(2,1)}, u32[]{:S(2)}) copy-start(bf16[320,2048]{1,0:T(8,128)(2,1)} %param.22) | copy-start | bytes 3932164
  62.1 108.4 %all-gather.5.cloned.1.call-start = ((), (), s32[]{:S(2)}) async-start(), calls=%async_computation.2 | async-start | bytes 7208960 | tf_op jit(solution)/shard_map/all_gather | solution.py:133
  62.6 214.1 %all-gather.7.cloned.1.call-start = ((), (), s32[]{:S(2)}) async-start(), calls=%async_computation.3 | async-start | bytes 7208960 | tf_op jit(solution)/shard_map/all_gather | solution.py:134
  63.2 319.8 %all-gather.9.cloned.1.call-start = ((), (), s32[]{:S(2)}) async-start(), calls=%async_computation.4 | async-start | bytes 7208960 | tf_op jit(solution)/shard_map/all_gather | solution.py:140
  63.8 106.7 %copy-start.4 = (f32[2048]{0:T(1024)S(1)}, f32[2048]{0:T(1024)}, u32[]{:S(2)}) copy-start(f32[2048]{0:T(1024)} %param.24) | copy-start | bytes 24580
  63.8 354.8 %reduce-scatter.2.cloned.1.call-start = ((), (), s32[]{:S(2)}) async-start(), calls=%async_computation.5 | async-start | bytes 1638400 | tf_op jit(solution)/shard_map/reduce_scatter | solution.py:143
Sparse Core Ops, SparseCore 0:
  62.2 38.9 all-reduce.1
  393.8 24.6 reduce-scatter.1
Sparse Core Ops, SparseCore 1:
  64.1 106.3 all-gather.4
  171.9 104.8 all-gather.6
  278.2 104.8 all-gather.8
where the time goes:
time: 428 us
  waiting for transfers between devices  336 us (79%)
  blocking collectives  31.9 us (7%)
  matrix products  31.9 us (7%)
  between operations  15.2 us (4%)
  other arithmetic  10.5 us (2%)
    all_gather x1, waiting for transfers between devices, local(): lax.all_gather(down_weight, 'sp', axis=1, tiled=True)  106 us
    all_gather x1, waiting for transfers between devices, local(): up_piece = lax.all_gather(up_weight, 'sp', axis=0, tiled=True)  99.7 us
    all_gather x1, waiting for transfers between devices, local(): gate_piece = lax.all_gather(gate_weight, 'sp', axis=0, tiled=True)  66.1 us
    psum x1, waiting for transfers between devices, local(): summed = lax.psum(projected, 'tp').astype(jnp.float32)  37.3 us
    reduce_scatter x1, waiting for transfers between devices, local(): lax.psum_scatter(terms.astype(jnp.bfloat16), 'tp', scatter_dimension=0, t...  24.8 us
    all_gather x1, blocking collectives, local(): latent_piece = lax.all_gather(latent, 'sp', axis=0, tiled=True)  16.8 us
    all_gather x1, blocking collectives, local(): rope_piece = lax.all_gather(key_turned, 'sp', axis=0, tiled=True)  15.1 us
    dot_general x1, matrix products, local(): jnp.dot(hidden, lax.all_gather(down_weight, 'sp', axis=1, tiled=True), pr...  10.7 us
  transfers between devices with their start and end apart: 5, of which 5 were waited for; matrix products, arithmetic and copies ran while one was open for 2% of the time, Pallas kernels for 0%

commit v1 on v0

--- a/solution.py
+++ b/solution.py
@@ -130,7 +130,12 @@
     mixed_all = residual.astype(jnp.float32) + summed
     normed_all = norm_rows(mixed_all, ffn_gain).astype(jnp.bfloat16)
     mixed_own = lax.dynamic_slice_in_dim(mixed_all, tp_index * own_rows, own_rows, 0)
-    gate_piece = lax.all_gather(gate_weight, "sp", axis=0, tiled=True)
+    ring = [gate_weight]
+    for hop in range(3):
+        ring.append(lax.ppermute(ring[-1], "sp", [(dev, (dev + 1) % 4) for dev in range(4)]))
+    gate_piece = jnp.roll(
+        jnp.concatenate(ring[::-1], axis=0), (lax.axis_index("sp") + 1) * ring[0].shape[0], axis=0
+    )
     up_piece = lax.all_gather(up_weight, "sp", axis=0, tiled=True)
     gate = jnp.dot(normed_all, gate_piece, preferred_element_type=jnp.float32)
     up_part = jnp.dot(normed_all, up_piece, preferred_element_type=jnp.float32)

time: 428 us -> 387 us (0.904)
  waiting for transfers between devices: 336 us -> 259 us
  starting transfers between devices: 0.17 us -> 18.3 us
  local copies, waits for them, and re-layouts: 2.49 us -> 19.2 us
    ppermute x0 -> x3, waiting for transfers between devices: none -> 177 us  [local(): lax.ppermute(ring[-1], 'sp', [(dev, (dev + 1) % 4) for dev in range(4)])]
    all_gather x1, waiting for transfers between devices: 99.7 us -> 0.01 us  [local(): up_piece = lax.all_gather(up_weight, 'sp', axis=0, tiled=True)]
    all_gather x1 -> x0, waiting for transfers between devices: 66.1 us -> none  [local(): gate_piece = lax.all_gather(gate_weight, 'sp', axis=0, tiled=True)]
    all_gather x1, waiting for transfers between devices: 106 us -> 56.2 us  [local(): lax.all_gather(down_weight, 'sp', axis=1, tiled=True)]
    psum x1, waiting for transfers between devices: 37.3 us -> 0.01 us  [local(): summed = lax.psum(projected, 'tp').astype(jnp.float32)]
    ppermute x0 -> x3, starting transfers between devices: none -> 18.1 us  [local(): lax.ppermute(ring[-1], 'sp', [(dev, (dev + 1) % 4) for dev in range(4)])]
    unnamed x11 -> x24, local copies, waits for them, and re-layouts: 1.29 us -> 16.8 us
  transfers between devices with their start and end apart: 5 -> 7, of which waited for: 5 -> 5; matrix products, arithmetic and copies ran while one was open for 2% -> 7% of each run, Pallas kernels for 0% -> 0%
where the time goes in v1:
time: 387 us
  waiting for transfers between devices  259 us (67%)
  matrix products  32.3 us (8%)
  blocking collectives  31.9 us (8%)
  local copies, waits for them, and re-layouts  19.2 us (5%)
  starting transfers between devices  18.3 us (5%)
  between operations  15 us (4%)
  other arithmetic  11 us (3%)
    ppermute x3, waiting for transfers between devices, local(): lax.ppermute(ring[-1], 'sp', [(dev, (dev + 1) % 4) for dev in range(4)])  177 us
    all_gather x1, waiting for transfers between devices, local(): lax.all_gather(down_weight, 'sp', axis=1, tiled=True)  56.2 us
    reduce_scatter x1, waiting for transfers between devices, local(): lax.psum_scatter(terms.astype(jnp.bfloat16), 'tp', scatter_dimension=0, t...  25.4 us
    ppermute x3, starting transfers between devices, local(): lax.ppermute(ring[-1], 'sp', [(dev, (dev + 1) % 4) for dev in range(4)])  18.1 us
    all_gather x1, blocking collectives, local(): latent_piece = lax.all_gather(latent, 'sp', axis=0, tiled=True)  16.8 us
    unnamed x24, local copies, waits for them, and re-layouts  16.8 us
    all_gather x1, blocking collectives, local(): rope_piece = lax.all_gather(key_turned, 'sp', axis=0, tiled=True)  15.1 us
    dot_general x1, matrix products, local(): jnp.dot(hidden, lax.all_gather(down_weight, 'sp', axis=1, tiled=True), pr...  10.6 us
  transfers between devices with their start and end apart: 7, of which 5 were waited for; matrix products, arithmetic and copies ran while one was open for 7% of the time, Pallas kernels for 0%

profile of v1, /device:TPU:0, one launch (start us, length us, event | category | flops | bytes accessed | tf_op | source)
XLA Modules:
  0.0 387.0 jit_solution(9562380086568254285)
XLA Ops:
  7.4 0.0 copy-start
  7.4 0.0 all-reduce.2.cloned.1.call-start
  7.4 1.1 copy.26
  8.6 0.7 convert.18
  9.3 0.2 multiply_cosine_fusion
  9.5 0.2 fusion.38
  9.7 15.1 %all-gather = bf16[4,320,32]{1,2,0:T(8,128)(2,1)S(1)} all-gather(bf16[1,320,32]{1,2,0:T(8,128)(2,1)S(1)} %bitcast.81), channel_id=1, replica_groups=mesh['grp'=2,'sp'=4,'tp'=4] {'sp'}, dimensions={0}, use_global_device_ids=true | all-gather | bytes 102400 | tf_op jit(solution)/shard_map/all_gather | solution.py:105
  24.8 0.1 copy.25
  24.8 0.1 reshape.160
  25.0 1.1 fusion.30
  26.1 1.0 fusion.32
  27.1 16.8 %all_gather.12 = bf16[1280,256]{1,0:T(8,128)(2,1)S(1)} all-gather(bf16[320,256]{1,0:T(8,128)(2,1)S(1)} %fusion.32), channel_id=1, replica_groups=mesh['grp'=2,'sp'=4,'tp'=4] {'sp'}, dimensions={0}, use_global_device_ids=true | all-gather | bytes 819200 | tf_op jit(solution)/shard_map/all_gather | solution.py:104
  43.9 0.0 copy-done.6
  43.9 0.2 copy.24
  44.2 1.0 constant_dynamic-slice_fusion
  45.2 15.2 %while.15 = (s32[]{:T(128)}, f32[4,320]{1,0:T(4,128)S(1)}, f32[4,320]{1,0:T(4,128)S(1)}, f32[320,4,64]{0,2,1:T(8,128)S(1)}, bf16[2,640,256]{2,1,0:T(8,128)(2,1)S...) while((s32[]{:T(128)}, f32[4,320]{1,0:T(4,128)S(1)}, ...), condition=%wide.region_4.5_spmd.clone, body=%wide.region_1.4_spmd.clone.sunk | while | flops 436231680 | bytes 32759976 | solution.py:119
  45.2 0.3 convolution_convert_fusion.6
  45.5 0.6 fusion.81
  46.1 2.4 fusion.82
  48.5 0.3 convolution_convert_fusion.7
  48.8 2.9 fusion.86
  51.8 0.0 copy-done.1
  51.8 1.0 fusion.84
  52.8 0.3 convolution_convert_fusion.6
  53.1 0.6 fusion.81
  53.7 2.4 fusion.82
  56.1 0.3 convolution_convert_fusion.7
  56.4 2.9 fusion.86
  59.3 0.0 copy-done.1
  59.4 1.0 fusion.84
  60.4 0.0 copy-done
  60.4 1.6 convolution_convert_fusion.3
  62.0 0.0 all-reduce.2.cloned.1.call-update
  62.0 0.0 all-gather.4.cloned.1.call-start
  62.1 0.5 all-gather.4.cloned.1.call-update
  62.6 0.0 all-gather.6.cloned.1.call-start
  62.7 0.5 all-gather.6.cloned.1.call-update
  63.2 0.0 reduce-scatter.2.cloned.1.call-start
  63.3 0.1 copy-done.2
  63.4 0.1 collective-permute-start
  63.5 52.6 %collective-permute-done = bf16[512,1408]{1,0:T(8,128)(2,1)S(1)} collective-permute-done((bf16[512,1408]{1,0:T(8,128)(2,1)S(1)}, bf16[512,1408]{1,0:T(8,128)(2,1)S(1)}, u32[]{:S(2)}, u32[]{:S(2)}) %collective-permute-start) | collective-permute-done | bytes 1441824 | tf_op jit(solution)/shard_map/ppermute | solution.py:135
  116.1 1.2 copy-done.3
  117.3 13.5 %collective-permute-start.1 = (bf16[512,1408]{1,0:T(8,128)(2,1)S(1)}, bf16[512,1408]{1,0:T(8,128)(2,1)}, u32[]{:S(2)}, u32[]{:S(2)}) collective-permute-start(bf16[512,1408]{1,0:T(8,128)(2,1)S(1)} %collective-permute-done), channel_id=1, source_target_pairs={{0,4},{4,8},{8,12},{12,0},{1,5},{5,9},{9,13},{13,1},{2,6},{6,10},{... | collective-permute-start | bytes 4325384 | tf_op jit(solution)/shard_map/ppermute | solution.py:135
  130.8 75.2 %collective-permute-done.1 = bf16[512,1408]{1,0:T(8,128)(2,1)} collective-permute-done((bf16[512,1408]{1,0:T(8,128)(2,1)S(1)}, bf16[512,1408]{1,0:T(8,128)(2,1)}, u32[]{:S(2)}, u32[]{:S(2)}) %collective-permute-start.1) | collective-permute-done | bytes 1441824 | tf_op jit(solution)/shard_map/ppermute | solution.py:135
  206.0 4.5 %collective-permute-start.2 = (bf16[512,1408]{1,0:T(8,128)(2,1)}, bf16[512,1408]{1,0:T(8,128)(2,1)}, u32[]{:S(2)}, u32[]{:S(2)}) collective-permute-start(bf16[512,1408]{1,0:T(8,128)(2,1)} %collective-permute-done.1), channel_id=1, source_target_pairs={{0,4},{4,8},{8,12},{12,0},{1,5},{5,9},{9,13},{13,1},{2,6},{6,10},{... | collective-permute-start | bytes 4325384 | tf_op jit(solution)/shard_map/ppermute | solution.py:135
  210.5 3.7 convert_add_fusion
  214.2 48.7 %collective-permute-done.2 = bf16[512,1408]{1,0:T(8,128)(2,1)} collective-permute-done((bf16[512,1408]{1,0:T(8,128)(2,1)}, bf16[512,1408]{1,0:T(8,128)(2,1)}, u32[]{:S(2)}, u32[]{:S(2)}) %collective-permute-start.2) | collective-permute-done | bytes 1441824 | tf_op jit(solution)/shard_map/ppermute | solution.py:135
  262.9 2.6 constant_dynamic-update-slice_fusion.7
  265.5 2.6 constant_dynamic-update-slice_fusion.6
  268.1 0.0 copy-done.4
  268.1 1.2 constant_dynamic-update-slice_fusion.5
  269.3 1.3 constant_dynamic-update-slice_fusion.4
  270.6 2.6 constant_dynamic-update-slice_fusion.3
  273.2 2.7 constant_dynamic-update-slice_fusion.2
  275.8 1.3 constant_dynamic-update-slice_fusion.1
  277.1 1.2 constant_dynamic-update-slice_fusion
  278.3 0.0 copy-done.7
  278.3 7.0 %fusion.44 = f32[320,1408]{1,0:T(8,128)} fusion(bf16[2048,1408]{1,0:T(8,128)(2,1)} %all-gather.4.cloned.1.call-done, f32[2048]{0:T(1024)S(1)} %copy-done.7, f32[320]{0:T(512)S(1)} %add_rsqrt_fusion, bf16[320,2048]{1,0:T(8,128)(2,1)} %all-reduce.2.cloned.1.call-done, bf16[320,2048]{1,0:T(8,128)(2,1)} %param.22), kind=kOutput, calls=%fused_computation.80 | convolution fusion | flops 1849425920 | bytes 10200320 | tf_op jit(solution)/shard_map/dot_general | solution.py:141
  285.4 56.2 %all-gather.6.cloned.1.call-done = bf16[1408,2048]{1,0:T(8,128)(2,1)} async-done(((bf16[1408,512]{1,0:T(8,128)(2,1)}), bf16[1408,2048]{1,0:T(8,128)(2,1)}) %all-gather.6.cloned.1.call-update) | async-done | bytes 5767184 | tf_op jit(solution)/shard_map/all_gather | solution.py:145
  341.6 0.0 copy-done.5
  341.6 10.6 %convolution_convert_fusion.2 = bf16[320,2048]{1,0:T(8,128)(2,1)} fusion(bf16[1408,2048]{1,0:T(8,128)(2,1)} %all-gather.6.cloned.1.call-done, f32[320,1408]{1,0:T(8,128)} %fusion.44, bf16[4096,1408]{1,0:T(8,128)(2,1)} %constant_dynamic-update-slice_fusion, s32[]{:T(128)S(6)} %select_n.57, f32[2048]{0:T(1024)S(1)} %copy-done.7, f32[320]{0:T(512)S(1)} %add_rsqrt_fusion, ...), kind=kOutput, calls=%fused_computation.28 | convolution fusion | flops 3698278400 | bytes 17278212 | tf_op jit(solution)/shard_map/dot_general | solution.py:143
  352.2 0.0 reduce-scatter.2.cloned.1.call-update
  352.2 25.4 %reduce-scatter.2.cloned.1.call-done = bf16[80,2048]{1,0:T(8,128)(2,1)} async-done(((bf16[320,2048]{1,0:T(8,128)(2,1)}), bf16[80,2048]{1,0:T(8,128)(2,1)}) %reduce-scatter.2.cloned.1.call-update) | async-done | bytes 327696 | tf_op jit(solution)/shard_map/reduce_scatter | solution.py:148
  377.6 2.0 add_convert_fusion
  (30 shorter events, 0.3 us)
Async XLA Ops:
  7.4 53.0 %copy-start = (bf16[256,2048]{1,0:T(8,128)(2,1)S(1)}, bf16[256,2048]{1,0:T(8,128)(2,1)}, u32[]{:S(2)}) copy-start(bf16[256,2048]{1,0:T(8,128)(2,1)} %param.23) | copy-start | bytes 3145732
  7.4 36.6 %copy-start.6 = (bf16[320,256]{1,0:T(8,128)(2,1)S(1)}, bf16[320,256]{1,0:T(8,128)(2,1)}, u32[]{:S(2)}) copy-start(bf16[320,256]{1,0:T(8,128)(2,1)} %param.15) | copy-start | bytes 491524
  7.4 203.1 %all-reduce.2.cloned.1.call-start = ((), (), s32[]{:S(2)}) async-start(), calls=%async_computation.1 | async-start | bytes 2621440 | tf_op jit(solution)/shard_map/psum | solution.py:129
  48.5 3.2 copy-start.1
  56.1 3.2 copy-start.1
  62.0 1.4 copy-start.2
  62.0 216.3 %all-gather.4.cloned.1.call-start = ((), (), s32[]{:S(2)}) async-start(), calls=%async_computation.2 | async-start | bytes 7208960 | tf_op jit(solution)/shard_map/all_gather | solution.py:139
  62.6 278.9 %all-gather.6.cloned.1.call-start = ((), (), s32[]{:S(2)}) async-start(), calls=%async_computation.3 | async-start | bytes 7208960 | tf_op jit(solution)/shard_map/all_gather | solution.py:145
  63.2 314.4 %reduce-scatter.2.cloned.1.call-start = ((), (), s32[]{:S(2)}) async-start(), calls=%async_computation.4 | async-start | bytes 1638400 | tf_op jit(solution)/shard_map/reduce_scatter | solution.py:148
  63.4 52.7 %collective-permute-start = (bf16[512,1408]{1,0:T(8,128)(2,1)S(1)}, bf16[512,1408]{1,0:T(8,128)(2,1)S(1)}, u32[]{:S(2)}, u32[]{:S(2)}) collective-permute-start(bf16[512,1408]{1,0:T(8,128)(2,1)S(1)} %copy-done.2), channel_id=1, source_target_pairs={{0,4},{4,8},{8,12},{12,0},{1,5},{5,9},{9,13},{13,1},{2,6},{6,10},{... | collective-permute-start | bytes 4325384 | tf_op jit(solution)/shard_map/ppermute | solution.py:135
  116.1 1.2 copy-start.3
  117.3 88.7 %collective-permute-start.1 = (bf16[512,1408]{1,0:T(8,128)(2,1)S(1)}, bf16[512,1408]{1,0:T(8,128)(2,1)}, u32[]{:S(2)}, u32[]{:S(2)}) collective-permute-start(bf16[512,1408]{1,0:T(8,128)(2,1)S(1)} %collective-permute-done), channel_id=1, source_target_pairs={{0,4},{4,8},{8,12},{12,0},{1,5},{5,9},{9,13},{13,1},{2,6},{6,10},{... | collective-permute-start | bytes 4325384 | tf_op jit(solution)/shard_map/ppermute | solution.py:135
  206.0 56.9 %collective-permute-start.2 = (bf16[512,1408]{1,0:T(8,128)(2,1)}, bf16[512,1408]{1,0:T(8,128)(2,1)}, u32[]{:S(2)}, u32[]{:S(2)}) collective-permute-start(bf16[512,1408]{1,0:T(8,128)(2,1)} %collective-permute-done.1), channel_id=1, source_target_pairs={{0,4},{4,8},{8,12},{12,0},{1,5},{5,9},{9,13},{13,1},{2,6},{6,10},{... | collective-permute-start | bytes 4325384 | tf_op jit(solution)/shard_map/ppermute | solution.py:135
  214.2 53.9 %copy-start.4 = (bf16[512,1408]{1,0:T(8,128)(2,1)S(1)}, bf16[512,1408]{1,0:T(8,128)(2,1)}, u32[]{:S(2)}) copy-start(bf16[512,1408]{1,0:T(8,128)(2,1)} %copy-done.3) | copy-start | bytes 4325380
  275.8 2.5 copy-start.7
  278.3 63.3 %copy-start.5 = (bf16[320,2048]{1,0:T(8,128)(2,1)S(1)}, bf16[320,2048]{1,0:T(8,128)(2,1)}, u32[]{:S(2)}) copy-start(bf16[320,2048]{1,0:T(8,128)(2,1)} %param.22) | copy-start | bytes 3932164
Sparse Core Ops, SparseCore 0:
  62.2 38.8 all-reduce.1
  352.3 25.2 reduce-scatter.1
Sparse Core Ops, SparseCore 1:
  64.1 160.0 all-gather.3
  225.6 115.9 all-gather.5
